TPU v7x, 32 devices: a whole 2x2x4 slice. The times are simulated.
32 devices in a mesh: kv: 4 (over y, x), tp: 8 (over z, core).
Axes of the slice: x: 2, y: 2, z: 4, core: 2. Of those that a mesh axis runs over, the one named last changes fastest.
Arguments:
- residual: bfloat16 [128, 4096], P(None, ('kv', 'tp')), may hold values from -20 to 20
- mixer_gain: float32 [4096], P('kv'), may hold values from 0.1 to 1.9
- w_query: bfloat16 [4096, 4096], P('kv', 'tp'), may hold values from -0.09375 to 0.09375
- w_forget: bfloat16 [4096, 4096], P('kv', 'tp'), may hold values from -0.09375 to 0.09375
- w_input: bfloat16 [4096, 4096], P('kv', 'tp'), may hold values from -0.09375 to 0.09375
- w_outgate: bfloat16 [4096, 4096], P('kv', 'tp'), may hold values from -0.09375 to 0.09375
- lower_bound: float32 [4096], P('tp'), may hold values from 0.3 to 0.97
- state: float32 [128, 32, 128, 128], P('kv', 'tp'), may hold values from -6 to 6
- head_gain: float32 [128], replicated, may hold values from 0.1 to 1.9
- w_mix_out: bfloat16 [4096, 4096], P('tp', 'kv'), may hold values from -0.09375 to 0.09375
- ffn_gain: float32 [4096], P('kv'), may hold values from 0.1 to 1.9
- w_gate: bfloat16 [4096, 10752], P('kv', 'tp'), may hold values from -0.09375 to 0.09375
- w_up: bfloat16 [4096, 10752], P('kv', 'tp'), may hold values from -0.09375 to 0.09375
- w_down: bfloat16 [10752, 4096], P('tp', 'kv'), may hold values from -0.0625 to 0.0625
Outputs:
- layer_out: bfloat16 [128, 4096], P(None, ('kv', 'tp'))
- new_state: float32 [128, 32, 128, 128], P('kv', 'tp')
All inputs are finite; a program needn't handle non-finite values.
Results may differ from a plain program's by a relative error of at most 0.015.
Values may be sent and summed in bfloat16 or wider, within the bound.
No kernel may reach another device: no remote copies, remote signals or barrier semaphores. Data moves between devices by JAX's collectives and lax.ppermute only.
A program may use at most 64 MiB of HBM per device.

v0:
```python
import jax
import jax.numpy as jnp
from jax import lax
from jax.sharding import PartitionSpec as P

D = 4096
DK = 128
DV = 128
EPS = 1e-06


def project_row(weight, piece):
    return jnp.dot(piece, weight, preferred_element_type=jnp.float32)


def channel_mix(rows_in, ffn_gain, w_gate, w_up, w_down):
    rows_float = rows_in.astype(jnp.float32)
    squares = jnp.sum(rows_float * rows_float, axis=1)
    scaled = (rows_float * ffn_gain).astype(jnp.bfloat16)
    gate = jnp.dot(scaled, w_gate, preferred_element_type=jnp.float32)
    upper = jnp.dot(scaled, w_up, preferred_element_type=jnp.float32)
    whole_total = lax.psum(squares, "kv")
    gate, upper = (
        lax.psum(gate.astype(jnp.bfloat16), "kv").astype(jnp.float32),
        lax.psum(upper.astype(jnp.bfloat16), "kv").astype(jnp.float32),
    )
    inverse = lax.rsqrt(whole_total / D + EPS)[:, None]
    hidden = (jax.nn.silu(gate * inverse) * (upper * inverse)).astype(jnp.bfloat16)
    terms = jnp.dot(hidden, w_down, preferred_element_type=jnp.float32)
    summed = lax.psum_scatter(
        terms.astype(jnp.bfloat16), "tp", scatter_dimension=1, tiled=True
    ).astype(jnp.float32)
    width = summed.shape[1]
    own = lax.dynamic_slice_in_dim(rows_float, lax.axis_index("tp") * width, width, 1)
    return (own + summed).astype(jnp.bfloat16)


def body(
    residual,
    mixer_gain,
    w_query,
    w_forget,
    w_input,
    w_outgate,
    lower_bound,
    state,
    head_gain,
    w_mix_out,
    ffn_gain,
    w_gate,
    w_up,
    w_down,
):
    local_seqs, local_heads = (state.shape[0], state.shape[1])
    rows = lax.all_gather(residual, "tp", axis=1, tiled=True)
    rows_float = rows.astype(jnp.float32)
    squares = jnp.sum(rows_float * rows_float, axis=1)
    scaled = (rows_float * mixer_gain).astype(jnp.bfloat16)
    part_query = jnp.dot(scaled, w_query, preferred_element_type=jnp.float32)
    part_forget = jnp.dot(scaled, w_forget, preferred_element_type=jnp.float32)
    part_value = jnp.dot(scaled, w_input, preferred_element_type=jnp.float32)
    part_gate = jnp.dot(scaled, w_outgate, preferred_element_type=jnp.float32)
    whole_total = lax.psum(squares, "kv")
    total = lax.dynamic_slice_in_dim(whole_total, lax.axis_index("kv") * local_seqs, local_seqs)
    part_query, part_forget, part_value, part_gate = (
        lax.psum_scatter(part_query, "kv", scatter_dimension=0, tiled=True),
        lax.psum_scatter(part_forget, "kv", scatter_dimension=0, tiled=True),
        lax.psum_scatter(part_value, "kv", scatter_dimension=0, tiled=True),
        lax.psum_scatter(part_gate, "kv", scatter_dimension=0, tiled=True),
    )
    inverse = lax.rsqrt(total / D + EPS)[:, None]
    bound = lower_bound.reshape(local_heads, DK)
    forget_raw = (part_forget * inverse).reshape(local_seqs, local_heads, DK)
    forget = bound + (1.0 - bound) * jax.nn.sigmoid(forget_raw)
    keyvec = (1.0 - bound) * jax.nn.sigmoid(-forget_raw)
    query = jax.nn.silu((part_query * inverse).reshape(local_seqs, local_heads, DK))
    values = (part_value * inverse).reshape(local_seqs, local_heads, DV)
    updated = forget[..., None] * state + keyvec[..., None] * values[:, :, None, :]
    head_out = jnp.einsum("shc,shce->she", query, updated, precision=lax.Precision.HIGHEST)
    inv_head = lax.rsqrt(jnp.mean(head_out * head_out, axis=2, keepdims=True) + EPS)
    out_gate = jax.nn.silu((part_gate * inverse).reshape(local_seqs, local_heads, DV))
    normed = (
        (head_out * inv_head * head_gain * out_gate)
        .reshape(local_seqs, local_heads * DV)
        .astype(jnp.bfloat16)
    )
    terms = project_row(w_mix_out, lax.all_gather(normed, "kv", axis=0, tiled=True))
    mixed = lax.psum(terms, "tp")
    after_mix = (rows_float + mixed).astype(jnp.bfloat16)
    layer_out = channel_mix(after_mix, ffn_gain, w_gate, w_up, w_down)
    return (layer_out, updated)


def solution(mesh):
    in_specs = (
        P(None, ("kv", "tp")),
        P("kv"),
        P("kv", "tp"),
        P("kv", "tp"),
        P("kv", "tp"),
        P("kv", "tp"),
        P("tp"),
        P("kv", "tp", None, None),
        P(),
        P("tp", "kv"),
        P("kv"),
        P("kv", "tp"),
        P("kv", "tp"),
        P("tp", "kv"),
    )
    out_specs = (P(None, ("kv", "tp")), P("kv", "tp", None, None))
    return jax.shard_map(body, mesh=mesh, in_specs=in_specs, out_specs=out_specs, check_vma=False)
```

profile of v0, /device:TPU:0, one launch (start us, length us, event | category | flops | bytes accessed | tf_op | source)
XLA Modules:
  0.0 312.9 jit_solution(12020792351462122957)
XLA Ops:
  7.2 0.0 copy-start
  7.2 0.0 copy-start.4
  7.2 0.0 reduce-scatter.10.cloned.1.call-start
  7.2 15.1 %all_gather.6 = bf16[128,1024]{1,0:T(8,128)(2,1)S(1)} all-gather(bf16[128,128]{1,0:T(8,128)(2,1)} %param.14), channel_id=1, replica_groups=mesh['kv'=4,'tp'=8] {'tp'}, dimensions={1}, use_global_device_ids=true | all-gather | bytes 294912 | tf_op jit(solution)/shard_map/all_gather | solution.py:55
  22.4 2.3 fusion.10
  24.6 0.0 reduce-scatter.10.cloned.1.call-update
  24.7 0.0 reduce-scatter.12.cloned.1.call-start
  24.7 2.2 fusion.8
  27.0 0.0 reduce-scatter.12.cloned.1.call-update
  27.0 0.0 reduce-scatter.14.cloned.1.call-start
  27.0 2.3 fusion.6
  29.3 0.0 reduce-scatter.14.cloned.1.call-update
  29.3 0.0 reduce-scatter.8.cloned.1.call-start
  29.4 2.3 fusion.12
  31.6 0.0 reduce-scatter.8.cloned.1.call-update
  31.7 0.0 all-reduce.4.cloned.1.call-start
  31.7 0.1 fusion.1
  31.8 9.9 %psum.35 = f32[128]{0:T(128)S(1)} all-reduce(f32[128]{0:T(128)S(1)} %fusion.1), channel_id=1, replica_groups=mesh['kv'=4,'tp'=8] {'kv'}, use_global_device_ids=true, to_apply=%region_2.0 | all-reduce | flops 128 | bytes 1024 | tf_op jit(solution)/shard_map/psum | solution.py:63
  41.8 0.1 add_rsqrt_fusion.2
  41.8 0.7 broadcast_subtract_fusion
  42.5 6.5 %reduce-scatter.10.cloned.1.call-done = f32[32,512]{1,0:T(8,128)} async-done(((f32[128,512]{1,0:T(8,128)}), f32[32,512]{1,0:T(8,128)}) %reduce-scatter.10.cloned.1.call-update) | async-done | bytes 65552 | tf_op jit(solution)/shard_map/reduce_scatter | solution.py:67
  49.0 27.1 %reduce-scatter.12.cloned.1.call-done = f32[32,512]{1,0:T(8,128)} async-done(((f32[128,512]{1,0:T(8,128)}), f32[32,512]{1,0:T(8,128)}) %reduce-scatter.12.cloned.1.call-update) | async-done | bytes 65552 | tf_op jit(solution)/shard_map/reduce_scatter | solution.py:68
  76.1 27.2 %reduce-scatter.14.cloned.1.call-done = f32[32,512]{1,0:T(8,128)} async-done(((f32[128,512]{1,0:T(8,128)}), f32[32,512]{1,0:T(8,128)}) %reduce-scatter.14.cloned.1.call-update) | async-done | bytes 65552 | tf_op jit(solution)/shard_map/reduce_scatter | solution.py:69
  103.3 27.0 %reduce-scatter.8.cloned.1.call-done = f32[32,512]{1,0:T(8,128)} async-done(((f32[128,512]{1,0:T(8,128)}), f32[32,512]{1,0:T(8,128)}) %reduce-scatter.8.cloned.1.call-update) | async-done | bytes 65552 | tf_op jit(solution)/shard_map/reduce_scatter | solution.py:66
  130.3 1.0 add_divide_fusion.1
  131.6 0.0 copy-done.4
  131.6 8.2 %multiply_add_fusion = f32[32,4,128,128]{3,2,1,0:T(8,128)S(1)} fusion(f32[32,4,128,128]{3,2,1,0:T(8,128)} %param.21, f32[32,4,128]{2,1,0:T(4,128)S(1)} %mul.164, f32[32,4,128]{2,1,0:T(4,128)S(1)} %bitcast.35, f32[32,4,128]{2,1,0:T(4,128)S(1)} %bitcast.34), kind=kLoop, calls=%fused_computation | loop fusion | flops 6291456 | bytes 16973824 | tf_op jit(solution)/shard_map/add | solution.py:78
  139.8 0.0 copy-start.1
  139.8 0.0 copy-start.5
  139.9 0.0 copy-start.2
  139.9 0.0 copy-start.3
  139.9 3.4 %copy-done.1 = f32[32,4,128,128]{3,2,1,0:T(8,128)} copy-done((f32[32,4,128,128]{3,2,1,0:T(8,128)}, f32[32,4,128,128]{3,2,1,0:T(8,128)S(1)}, u32[]{:S(2)}) %copy-start.1) | copy-done | bytes 8388632
  143.2 7.2 %fusion.18 = f32[32,4,1,128]{3,2,1,0:T(1,128)S(1)} fusion(f32[32,4,128,1]{2,3,1,0:T(1,128)S(1)} %bitcast.33, f32[32,4,128,128]{3,2,1,0:T(8,128)S(1)} %multiply_add_fusion), kind=kOutput, calls=%fused_computation.39 | convolution fusion | flops 25165824 | bytes 8519680 | tf_op jit(solution)/shard_map/shc,shce->she/dot_general | solution.py:79
  150.5 0.1 multiply_reduce_fusion.1
  150.6 0.0 copy-done.5
  150.6 0.1 fusion.15
  150.8 8.5 %all_gather.7 = bf16[128,512]{1,0:T(8,128)(2,1)S(1)} all-gather(bf16[32,512]{1,0:T(8,128)(2,1)S(1)} %bitcast.38), channel_id=1, replica_groups=mesh['kv'=4,'tp'=8] {'kv'}, dimensions={0}, use_global_device_ids=true | all-gather | bytes 163840 | tf_op jit(solution)/shard_map/all_gather | solution.py:87
  159.2 0.0 copy-done.2
  159.2 1.1 fusion.19
  160.4 0.0 all-reduce.4.cloned.1.call-update
  160.4 0.0 all-reduce.6.cloned.1.call-start
  160.4 56.7 %all-reduce.4.cloned.1.call-done = f32[128,1024]{1,0:T(8,128)} async-done(((f32[128,1024]{1,0:T(8,128)}), f32[128,1024]{1,0:T(8,128)}) %all-reduce.4.cloned.1.call-update) | async-done | bytes 524304 | tf_op jit(solution)/shard_map/psum | solution.py:88
  217.1 1.2 multiply_reduce_fusion
  218.3 0.0 copy-done
  218.3 0.0 copy-done.3
  218.3 1.6 convolution_convert_fusion
  219.9 3.4 %convolution_convert_fusion.1 = bf16[128,1344]{0,1:T(8,128)(2,1)} fusion(bf16[1024,1344]{0,1:T(8,128)(2,1)} %param.25, f32[128,1024]{1,0:T(8,128)S(1)} %get-tuple-element.5, f32[1024]{0:T(1024)S(1)} %copy-done.3), kind=kOutput, calls=%fused_computation.2 | convolution fusion | flops 352755712 | bytes 3624960 | tf_op jit(solution)/shard_map/dot_general | solution.py:20
  223.3 0.0 all-reduce.6.cloned.1.call-update
  223.4 0.0 reduce-scatter.16.cloned.1.call-start
  223.4 10.2 %psum.38 = f32[128]{0:T(128)S(1)} all-reduce(f32[128]{0:T(128)S(1)} %get-tuple-element.4), channel_id=1, replica_groups=mesh['kv'=4,'tp'=8] {'kv'}, use_global_device_ids=true, to_apply=%region_10.11 | all-reduce | flops 128 | bytes 1024 | tf_op jit(solution)/shard_map/psum | solution.py:22
  233.6 36.4 %all-reduce.6.cloned.1.call-done = (bf16[128,1344]{0,1:T(8,128)(2,1)}, bf16[128,1344]{0,1:T(8,128)(2,1)}) async-done(((bf16[128,1344]{0,1:T(8,128)(2,1)}, bf16[128,1344]{0,1:T(8,128)(2,1)}), (bf16[128,1344]{0,1:T(8,128)(2,1)}, bf16[128,1344]{0,1:T(8,128)(2,1)})) %all-reduce.6.cloned.1.call-update) | async-done | bytes 688144 | tf_op jit(solution)/shard_map/psum | solution.py:25
  270.0 2.8 convolution_convert_fusion.2
  272.7 0.8 copy.18
  273.6 0.0 reduce-scatter.16.cloned.1.call-update
  273.6 31.0 %reduce-scatter.16.cloned.1.call-done = bf16[128,128]{1,0:T(8,128)(2,1)} async-done(((bf16[1024,128]{1,0:T(8,128)(2,1)}), bf16[128,128]{1,0:T(8,128)(2,1)}) %reduce-scatter.16.cloned.1.call-update) | async-done | bytes 32784
  304.5 0.9 copy.19
  305.4 0.6 add_convert_fusion
  (12 shorter events, 0.2 us)
Async XLA Ops:
  7.2 211.1 %copy-start = (bf16[1024,1344]{0,1:T(8,128)(2,1)S(1)}, bf16[1024,1344]{0,1:T(8,128)(2,1)}, u32[]{:S(2)}) copy-start(bf16[1024,1344]{0,1:T(8,128)(2,1)} %param.26) | copy-start | bytes 8257540
  7.2 124.4 %copy-start.4 = (f32[512]{0:T(512)S(1)}, f32[512]{0:T(512)}, u32[]{:S(2)}) copy-start(f32[512]{0:T(512)} %param.20) | copy-start | bytes 6148
  7.2 41.8 %reduce-scatter.10.cloned.1.call-start = ((), (), s32[]{:S(2)}) async-start(), calls=%async_computation.6 | async-start | bytes 327680 | tf_op jit(solution)/shard_map/reduce_scatter | solution.py:67
  24.7 51.5 %reduce-scatter.12.cloned.1.call-start = ((), (), s32[]{:S(2)}) async-start(), calls=%async_computation.7 | async-start | bytes 327680 | tf_op jit(solution)/shard_map/reduce_scatter | solution.py:68
  27.0 76.3 %reduce-scatter.14.cloned.1.call-start = ((), (), s32[]{:S(2)}) async-start(), calls=%async_computation.8 | async-start | bytes 327680 | tf_op jit(solution)/shard_map/reduce_scatter | solution.py:69
  29.3 101.0 %reduce-scatter.8.cloned.1.call-start = ((), (), s32[]{:S(2)}) async-start(), calls=%async_computation.5 | async-start | bytes 327680 | tf_op jit(solution)/shard_map/reduce_scatter | solution.py:66
  31.7 185.4 %all-reduce.4.cloned.1.call-start = ((), (), s32[]{:S(2)}) async-start(), calls=%async_computation.9 | async-start | bytes 1048576 | tf_op jit(solution)/shard_map/psum | solution.py:88
  139.8 3.4 %copy-start.1 = (f32[32,4,128,128]{3,2,1,0:T(8,128)}, f32[32,4,128,128]{3,2,1,0:T(8,128)S(1)}, u32[]{:S(2)}) copy-start(f32[32,4,128,128]{3,2,1,0:T(8,128)S(1)} %multiply_add_fusion) | copy-start | bytes 25165828
  139.8 10.8 %copy-start.5 = (f32[128]{0:T(128)S(1)}, f32[128]{0:T(128)}, u32[]{:S(2)}) copy-start(f32[128]{0:T(128)} %param.22) | copy-start | bytes 1540
  139.9 19.4 %copy-start.2 = (bf16[512,1024]{1,0:T(8,128)(2,1)S(1)}, bf16[512,1024]{1,0:T(8,128)(2,1)}, u32[]{:S(2)}) copy-start(bf16[512,1024]{1,0:T(8,128)(2,1)} %param.23) | copy-start | bytes 3145732
  139.9 78.4 %copy-start.3 = (f32[1024]{0:T(1024)S(1)}, f32[1024]{0:T(1024)}, u32[]{:S(2)}) copy-start(f32[1024]{0:T(1024)} %param.24) | copy-start | bytes 12292
  160.4 109.6 %all-reduce.6.cloned.1.call-start = ((), (), s32[]{:S(2)}) async-start(), calls=%async_computation.11 | async-start | bytes 1376256 | tf_op jit(solution)/shard_map/psum | solution.py:25
  223.4 81.2 %reduce-scatter.16.cloned.1.call-start = ((), (), s32[]{:S(2)}) async-start(), calls=%async_computation.10 | async-start | bytes 294912
Sparse Core Ops, SparseCore 0:
  24.8 24.1 reduce-scatter.9
  51.7 24.3 reduce-scatter.11
  78.9 24.3 reduce-scatter.13
  105.9 24.3 reduce-scatter.7
  160.5 56.5 all-reduce.3
  223.5 46.4 all-reduce.5
  273.7 30.7 reduce-scatter.15
where the time goes:
time: 314 us; the launch traced here: 313 us
  waiting for transfers between devices  212 us (68%)
  blocking collectives  43.7 us (14%)
  matrix products  25.2 us (8%)
  between operations  14.3 us (5%)
  other arithmetic  12.3 us (4%)
  local copies, waits for them, and re-layouts  5.22 us (2%)
    psum x1, waiting for transfers between devices, body(): mixed = lax.psum(terms, 'tp')  56.7 us
    psum x1, waiting for transfers between devices, channel_mix(): lax.psum(upper.astype(jnp.bfloat16), 'kv').astype(jnp.float32)  36.4 us
    unnamed x8, waiting for transfers between devices  31.1 us
    reduce_scatter x1, waiting for transfers between devices, body(): lax.psum_scatter(part_gate, 'kv', scatter_dimension=0, tiled=True)  27.2 us
    reduce_scatter x1, waiting for transfers between devices, body(): lax.psum_scatter(part_value, 'kv', scatter_dimension=0, tiled=True)  27.1 us
    reduce_scatter x1, waiting for transfers between devices, body(): lax.psum_scatter(part_query, 'kv', scatter_dimension=0, tiled=True)  27 us
    all_gather x1, blocking collectives, body(): rows = lax.all_gather(residual, 'tp', axis=1, tiled=True)  15.1 us
    psum x1, blocking collectives, channel_mix(): whole_total = lax.psum(squares, 'kv')  10.2 us
  transfers between devices with their start and end apart: 7, of which 7 were waited for; matrix products, arithmetic and copies ran while one was open for 2% of the time, Pallas kernels for 0%

commit v1 on v0

--- a/solution.py
+++ b/solution.py
@@ -85,7 +85,9 @@
         .astype(jnp.bfloat16)
     )
     terms = project_row(w_mix_out, lax.all_gather(normed, "kv", axis=0, tiled=True))
-    mixed = lax.psum(terms, "tp")
+    mixed = terms
+    for hop in (1, 2, 4):
+        mixed = mixed + lax.ppermute(mixed, "tp", [(dev, dev ^ hop) for dev in range(8)])
     after_mix = (rows_float + mixed).astype(jnp.bfloat16)
     layer_out = channel_mix(after_mix, ffn_gain, w_gate, w_up, w_down)
     return (layer_out, updated)

time: 314 us -> 292 us (0.930)
  waiting for transfers between devices: 212 us -> 194 us
  starting transfers between devices: 0.29 us -> 4.34 us
  local copies, waits for them, and re-layouts: 5.22 us -> 1.87 us
    psum x1 -> x0, waiting for transfers between devices: 56.7 us -> none  [body(): mixed = lax.psum(terms, 'tp')]
    ppermute x0 -> x3, waiting for transfers between devices: none -> 37.2 us  [body(): lax.ppermute(mixed, 'tp', [(dev, dev ^ hop) for dev in range(8)])]
    ppermute x0 -> x3, starting transfers between devices: none -> 4.09 us  [body(): lax.ppermute(mixed, 'tp', [(dev, dev ^ hop) for dev in range(8)])]
    unnamed x17 -> x19, local copies, waits for them, and re-layouts: 5.09 us -> 1.75 us
    unnamed x8 -> x7, waiting for transfers between devices: 31.1 us -> 31.1 us
  transfers between devices with their start and end apart: 7 -> 9, of which waited for: 7 -> 9; matrix products, arithmetic and copies ran while one was open for 2% -> 3% of each run, Pallas kernels for 0% -> 0%
where the time goes in v1:
time: 292 us
  waiting for transfers between devices  194 us (66%)
  blocking collectives  42.6 us (15%)
  matrix products  22.6 us (8%)
  between operations  14.4 us (5%)
  other arithmetic  11.4 us (4%)
  starting transfers between devices  4.34 us (1%)
    psum x1, waiting for transfers between devices, channel_mix(): lax.psum(upper.astype(jnp.bfloat16), 'kv').astype(jnp.float32)  38.4 us
    ppermute x3, waiting for transfers between devices, body(): lax.ppermute(mixed, 'tp', [(dev, dev ^ hop) for dev in range(8)])  37.2 us
    unnamed x7, waiting for transfers between devices  31.1 us
    reduce_scatter x1, waiting for transfers between devices, body(): lax.psum_scatter(part_gate, 'kv', scatter_dimension=0, tiled=True)  27.2 us
    reduce_scatter x1, waiting for transfers between devices, body(): lax.psum_scatter(part_value, 'kv', scatter_dimension=0, tiled=True)  27.1 us
    reduce_scatter x1, waiting for transfers between devices, body(): lax.psum_scatter(part_query, 'kv', scatter_dimension=0, tiled=True)  27 us
    all_gather x1, blocking collectives, body(): rows = lax.all_gather(residual, 'tp', axis=1, tiled=True)  15.1 us
    psum x1, blocking collectives, body(): whole_total = lax.psum(squares, 'kv')  9.9 us
  transfers between devices with their start and end apart: 9, of which 9 were waited for; matrix products, arithmetic and copies ran while one was open for 3% of the time, Pallas kernels for 0%

profile of v1, /device:TPU:0, one launch (start us, length us, event | category | flops | bytes accessed | tf_op | source)
XLA Modules:
  0.0 291.6 jit_solution(11257893826951274100)
XLA Ops:
  7.2 0.0 copy-start
  7.2 0.0 copy-start.5
  7.2 0.0 reduce-scatter.10.cloned.1.call-start
  7.2 15.1 %all_gather.6 = bf16[128,1024]{1,0:T(8,128)(2,1)S(1)} all-gather(bf16[128,128]{1,0:T(8,128)(2,1)} %param.14), channel_id=1, replica_groups=mesh['kv'=4,'tp'=8] {'tp'}, dimensions={1}, use_global_device_ids=true | all-gather | bytes 294912 | tf_op jit(solution)/shard_map/all_gather | solution.py:55
  22.4 2.3 fusion.10
  24.6 0.0 reduce-scatter.10.cloned.1.call-update
  24.7 0.0 reduce-scatter.12.cloned.1.call-start
  24.7 2.2 fusion.8
  27.0 0.0 reduce-scatter.12.cloned.1.call-update
  27.0 0.0 reduce-scatter.14.cloned.1.call-start
  27.0 2.3 fusion.6
  29.3 0.0 reduce-scatter.14.cloned.1.call-update
  29.3 0.0 reduce-scatter.8.cloned.1.call-start
  29.4 2.2 fusion.12
  31.6 0.0 reduce-scatter.8.cloned.1.call-update
  31.6 0.0 all-reduce.3.cloned.1.call-start
  31.7 0.1 fusion.1
  31.8 9.9 %psum.28 = f32[128]{0:T(128)S(1)} all-reduce(f32[128]{0:T(128)S(1)} %fusion.1), channel_id=1, replica_groups=mesh['kv'=4,'tp'=8] {'kv'}, use_global_device_ids=true, to_apply=%region_2.0 | all-reduce | flops 128 | bytes 1024 | tf_op jit(solution)/shard_map/psum | solution.py:63
  41.7 0.1 add_rsqrt_fusion.2
  41.8 0.7 broadcast_subtract_fusion
  42.5 6.5 %reduce-scatter.10.cloned.1.call-done = f32[32,512]{1,0:T(8,128)} async-done(((f32[128,512]{1,0:T(8,128)}), f32[32,512]{1,0:T(8,128)}) %reduce-scatter.10.cloned.1.call-update) | async-done | bytes 65552 | tf_op jit(solution)/shard_map/reduce_scatter | solution.py:67
  49.0 27.1 %reduce-scatter.12.cloned.1.call-done = f32[32,512]{1,0:T(8,128)} async-done(((f32[128,512]{1,0:T(8,128)}), f32[32,512]{1,0:T(8,128)}) %reduce-scatter.12.cloned.1.call-update) | async-done | bytes 65552 | tf_op jit(solution)/shard_map/reduce_scatter | solution.py:68
  76.1 27.2 %reduce-scatter.14.cloned.1.call-done = f32[32,512]{1,0:T(8,128)} async-done(((f32[128,512]{1,0:T(8,128)}), f32[32,512]{1,0:T(8,128)}) %reduce-scatter.14.cloned.1.call-update) | async-done | bytes 65552 | tf_op jit(solution)/shard_map/reduce_scatter | solution.py:69
  103.3 27.0 %reduce-scatter.8.cloned.1.call-done = f32[32,512]{1,0:T(8,128)} async-done(((f32[128,512]{1,0:T(8,128)}), f32[32,512]{1,0:T(8,128)}) %reduce-scatter.8.cloned.1.call-update) | async-done | bytes 65552 | tf_op jit(solution)/shard_map/reduce_scatter | solution.py:66
  130.3 1.0 add_divide_fusion.1
  131.6 0.0 copy-done.5
  131.6 8.2 %multiply_add_fusion = f32[32,4,128,128]{3,2,1,0:T(8,128)S(1)} fusion(f32[32,4,128,128]{3,2,1,0:T(8,128)} %param.21, f32[32,4,128]{2,1,0:T(4,128)S(1)} %mul.164, f32[32,4,128]{2,1,0:T(4,128)S(1)} %bitcast.35, f32[32,4,128]{2,1,0:T(4,128)S(1)} %bitcast.34), kind=kLoop, calls=%fused_computation | loop fusion | flops 6291456 | bytes 16973824 | tf_op jit(solution)/shard_map/add | solution.py:78
  139.8 0.0 copy-start.1
  139.8 0.0 copy-start.6
  139.9 0.0 copy-start.3
  139.9 0.0 copy-start.4
  139.9 0.0 copy-start.2
  139.9 7.2 %fusion.18 = f32[32,4,1,128]{3,2,1,0:T(1,128)S(1)} fusion(f32[32,4,128,1]{2,3,1,0:T(1,128)S(1)} %bitcast.33, f32[32,4,128,128]{3,2,1,0:T(8,128)S(1)} %multiply_add_fusion), kind=kOutput, calls=%fused_computation.39 | convolution fusion | flops 25165824 | bytes 8519680 | tf_op jit(solution)/shard_map/shc,shce->she/dot_general | solution.py:79
  147.1 0.1 multiply_reduce_fusion.1
  147.3 0.0 copy-done.6
  147.3 0.1 fusion.15
  147.4 8.5 %all_gather.7 = bf16[128,512]{1,0:T(8,128)(2,1)S(1)} all-gather(bf16[32,512]{1,0:T(8,128)(2,1)S(1)} %bitcast.38), channel_id=1, replica_groups=mesh['kv'=4,'tp'=8] {'kv'}, dimensions={0}, use_global_device_ids=true | all-gather | bytes 163840 | tf_op jit(solution)/shard_map/all_gather | solution.py:87
  155.9 0.0 copy-done.3
  155.9 0.3 fusion.19
  156.2 0.1 collective-permute-start
  156.3 1.9 collective-permute-done
  158.2 0.1 add.119
  158.3 1.6 collective-permute-start.1
  159.8 12.5 %collective-permute-done.1 = f32[128,1024]{1,0:T(8,128)S(1)} collective-permute-done((f32[128,1024]{1,0:T(8,128)S(1)}, f32[128,1024]{1,0:T(8,128)S(1)}, u32[]{:S(2)}, u32[]{:S(2)}) %collective-permute-start.1) | collective-permute-done | bytes 524320 | tf_op jit(solution)/shard_map/ppermute | solution.py:90
  172.3 0.1 add.120
  172.4 2.5 collective-permute-start.2
  174.8 22.8 %collective-permute-done.2 = f32[128,1024]{1,0:T(8,128)S(1)} collective-permute-done((f32[128,1024]{1,0:T(8,128)S(1)}, f32[128,1024]{1,0:T(8,128)S(1)}, u32[]{:S(2)}, u32[]{:S(2)}) %collective-permute-start.2) | collective-permute-done | bytes 524320 | tf_op jit(solution)/shard_map/ppermute | solution.py:90
  197.7 0.2 multiply_reduce_fusion
  197.8 0.0 copy-done
  197.8 0.0 copy-done.4
  197.8 1.6 convolution_convert_fusion
  199.5 0.0 copy-done.1
  199.5 0.0 copy-done.2
  199.5 1.6 convolution_convert_fusion.1
  201.1 0.0 all-reduce.3.cloned.1.call-update
  201.1 0.0 reduce-scatter.16.cloned.1.call-start
  201.2 9.0 %psum.30 = f32[128]{0:T(128)S(1)} all-reduce(f32[128]{0:T(128)S(1)} %get-tuple-element.4), channel_id=1, replica_groups=mesh['kv'=4,'tp'=8] {'kv'}, use_global_device_ids=true, to_apply=%region_9.10 | all-reduce | flops 128 | bytes 1024 | tf_op jit(solution)/shard_map/psum | solution.py:22
  210.2 38.4 %all-reduce.3.cloned.1.call-done = (bf16[128,1344]{0,1:T(8,128)(2,1)}, bf16[128,1344]{0,1:T(8,128)(2,1)}) async-done(((bf16[128,1344]{0,1:T(8,128)(2,1)}, bf16[128,1344]{0,1:T(8,128)(2,1)}), (bf16[128,1344]{0,1:T(8,128)(2,1)}, bf16[128,1344]{0,1:T(8,128)(2,1)})) %all-reduce.3.cloned.1.call-update) | async-done | bytes 688144 | tf_op jit(solution)/shard_map/psum | solution.py:25
  248.6 2.8 convolution_convert_fusion.2
  251.4 0.8 copy.18
  252.2 0.0 reduce-scatter.16.cloned.1.call-update
  252.3 31.0 %reduce-scatter.16.cloned.1.call-done = bf16[128,128]{1,0:T(8,128)(2,1)} async-done(((bf16[1024,128]{1,0:T(8,128)(2,1)}), bf16[128,128]{1,0:T(8,128)(2,1)}) %reduce-scatter.16.cloned.1.call-update) | async-done | bytes 32784
  283.2 0.9 copy.19
  284.1 0.6 add_convert_fusion
  (12 shorter events, 0.2 us)
Async XLA Ops:
  7.2 190.7 %copy-start = (bf16[1024,1344]{0,1:T(8,128)(2,1)S(1)}, bf16[1024,1344]{0,1:T(8,128)(2,1)}, u32[]{:S(2)}) copy-start(bf16[1024,1344]{0,1:T(8,128)(2,1)} %param.26) | copy-start | bytes 8257540
  7.2 124.4 %copy-start.5 = (f32[512]{0:T(512)S(1)}, f32[512]{0:T(512)}, u32[]{:S(2)}) copy-start(f32[512]{0:T(512)} %param.20) | copy-start | bytes 6148
  7.2 41.8 %reduce-scatter.10.cloned.1.call-start = ((), (), s32[]{:S(2)}) async-start(), calls=%async_computation.6 | async-start | bytes 327680 | tf_op jit(solution)/shard_map/reduce_scatter | solution.py:67
  24.7 51.5 %reduce-scatter.12.cloned.1.call-start = ((), (), s32[]{:S(2)}) async-start(), calls=%async_computation.7 | async-start | bytes 327680 | tf_op jit(solution)/shard_map/reduce_scatter | solution.py:68
  27.0 76.3 %reduce-scatter.14.cloned.1.call-start = ((), (), s32[]{:S(2)}) async-start(), calls=%async_computation.8 | async-start | bytes 327680 | tf_op jit(solution)/shard_map/reduce_scatter | solution.py:69
  29.3 101.0 %reduce-scatter.8.cloned.1.call-start = ((), (), s32[]{:S(2)}) async-start(), calls=%async_computation.5 | async-start | bytes 327680 | tf_op jit(solution)/shard_map/reduce_scatter | solution.py:66
  31.6 217.0 %all-reduce.3.cloned.1.call-start = ((), (), s32[]{:S(2)}) async-start(), calls=%async_computation.10 | async-start | bytes 1376256 | tf_op jit(solution)/shard_map/psum | solution.py:25
  139.8 59.6 %copy-start.1 = (f32[32,4,128,128]{3,2,1,0:T(8,128)}, f32[32,4,128,128]{3,2,1,0:T(8,128)S(1)}, u32[]{:S(2)}) copy-start(f32[32,4,128,128]{3,2,1,0:T(8,128)S(1)} %multiply_add_fusion) | copy-start | bytes 25165828
  139.8 7.4 %copy-start.6 = (f32[128]{0:T(128)S(1)}, f32[128]{0:T(128)}, u32[]{:S(2)}) copy-start(f32[128]{0:T(128)} %param.22) | copy-start | bytes 1540
  139.9 16.0 %copy-start.3 = (bf16[512,1024]{1,0:T(8,128)(2,1)S(1)}, bf16[512,1024]{1,0:T(8,128)(2,1)}, u32[]{:S(2)}) copy-start(bf16[512,1024]{1,0:T(8,128)(2,1)} %param.23) | copy-start | bytes 3145732
  139.9 58.0 %copy-start.4 = (f32[1024]{0:T(1024)S(1)}, f32[1024]{0:T(1024)}, u32[]{:S(2)}) copy-start(f32[1024]{0:T(1024)} %param.24) | copy-start | bytes 12292
  139.9 59.6 %copy-start.2 = (bf16[1024,1344]{0,1:T(8,128)(2,1)S(1)}, bf16[1024,1344]{0,1:T(8,128)(2,1)}, u32[]{:S(2)}) copy-start(bf16[1024,1344]{0,1:T(8,128)(2,1)} %param.25) | copy-start | bytes 8257540
  156.2 2.0 collective-permute-start
  158.3 14.0 %collective-permute-start.1 = (f32[128,1024]{1,0:T(8,128)S(1)}, f32[128,1024]{1,0:T(8,128)S(1)}, u32[]{:S(2)}, u32[]{:S(2)}) collective-permute-start(f32[128,1024]{1,0:T(8,128)S(1)} %add.119), channel_id=1, source_target_pairs={{0,2},{1,3},{2,0},{3,1},{4,6},{5,7},{6,4},{7,5},{8,10},{9,11},{10,... | collective-permute-start | bytes 1572872 | tf_op jit(solution)/shard_map/ppermute | solution.py:90
  172.4 25.3 %collective-permute-start.2 = (f32[128,1024]{1,0:T(8,128)S(1)}, f32[128,1024]{1,0:T(8,128)S(1)}, u32[]{:S(2)}, u32[]{:S(2)}) collective-permute-start(f32[128,1024]{1,0:T(8,128)S(1)} %add.120), channel_id=1, source_target_pairs={{0,4},{1,5},{2,6},{3,7},{4,0},{5,1},{6,2},{7,3},{8,12},{9,13},{10,... | collective-permute-start | bytes 1572872 | tf_op jit(solution)/shard_map/ppermute | solution.py:90
  201.1 82.1 %reduce-scatter.16.cloned.1.call-start = ((), (), s32[]{:S(2)}) async-start(), calls=%async_computation.9 | async-start | bytes 294912
Sparse Core Ops, SparseCore 0:
  24.8 24.1 reduce-scatter.9
  51.7 24.3 reduce-scatter.11
  78.9 24.3 reduce-scatter.13
  105.9 24.3 reduce-scatter.7
  201.3 47.3 all-reduce.2
  252.4 30.7 reduce-scatter.15
